TPU v7x, 256 devices: a whole 4x4x8 slice. The times are simulated.
256 devices in a mesh: ep: 32 (over z, x), tp: 8 (over y, core).
Axes of the slice: x: 4, y: 4, z: 8, core: 2. Of those that a mesh axis runs over, the one named last changes fastest.
Arguments:
- stream: bfloat16 [512, 4096], P(None, 'ep'), may hold values from -6.5 to 6.5
- norm_gain: float32 [4096], P('ep'), may hold values from 0.1 to 1.9
- w_query: bfloat16 [4096, 2048], P('ep', 'tp'), may hold values from -0.09375 to 0.09375
- w_key: bfloat16 [4096, 1024], P('ep', 'tp'), may hold values from -0.09375 to 0.09375
- w_value: bfloat16 [4096, 1024], P('ep', 'tp'), may hold values from -0.09375 to 0.09375
- break_offset: float32 [16], P('tp'), may hold values from -10 to -2
- cache_keys: bfloat16 [512, 1024, 8, 128], P('ep', None, 'tp'), may hold values from -6 to 6
- cache_values: bfloat16 [512, 1024, 8, 128], P('ep', None, 'tp'), may hold values from -6 to 6
- lengths: int32 [512], P('ep'), may hold values from 128 to 1024
- w_output: bfloat16 [2048, 4096], P('tp', 'ep'), may hold values from -0.125 to 0.125
- head_gain: float32 [2048], P('tp'), may hold values from 0.1 to 1.9
- ffn_gain: float32 [4096], P('ep'), may hold values from 0.1 to 1.9
- route_experts: int32 [512, 2], replicated, may hold values from 0 to 31, all different within a row; in each aligned block of 512 rows (0 to 511, 512 to 1023, ...) at most 64 rows name the same one
- route_weights: float32 [512, 2], replicated, may hold values from 0.1 to 1
- expert_gate: bfloat16 [32, 4096, 1024], P('ep', None, 'tp'), may hold values from -0.09375 to 0.09375
- expert_up: bfloat16 [32, 4096, 1024], P('ep', None, 'tp'), may hold values from -0.09375 to 0.09375
- expert_down: bfloat16 [32, 1024, 4096], P('ep', 'tp'), may hold values from -0.1875 to 0.1875
- dense_gate: bfloat16 [4096, 4096], P('ep', 'tp'), may hold values from -0.09375 to 0.09375
- dense_up: bfloat16 [4096, 4096], P('ep', 'tp'), may hold values from -0.09375 to 0.09375
- dense_down: bfloat16 [4096, 4096], P('tp', 'ep'), may hold values from -0.09375 to 0.09375
- mix_gain: float32 [4096], P('ep'), may hold values from 0.1 to 1.9
Outputs:
- mixed_out: bfloat16 [512, 4096], P(None, 'ep')
- key_rows: bfloat16 [512, 1024], P('ep', 'tp')
- value_rows: bfloat16 [512, 1024], P('ep', 'tp')
Inputs may be any that keep to these rules, and one draw needn't show every extreme that they name: `route_experts`: in the whole batch no expert is named by more than 64 pairs, a bound that some block reaches; the 2 experts of a token differ.
All inputs are finite; a program needn't handle non-finite values.
Results may differ from a plain program's by a relative error of at most 0.025.
Values may be sent and summed in bfloat16 or wider, within the bound.
A program may use at most 64 MiB of HBM per device.

v0:
```python
import jax
import jax.numpy as jnp
from jax import lax
from jax.sharding import PartitionSpec as P

EPSILON = 1e-06


def sent_to_all(x, axis):
    size = lax.axis_size(axis)
    return lax.all_to_all(jnp.broadcast_to(x[None], (size, *x.shape)), axis, 0, 0, tiled=True)


def taken_together(x, axis):
    return sent_to_all(x, axis).sum(axis=0)


def split_up(x, dim, size):
    lengths = x.shape
    blocks = x.reshape(*lengths[:dim], size, lengths[dim] // size, *lengths[dim + 1 :])
    return jnp.moveaxis(blocks, dim, 0)


def sent_and_summed(x, axis, dim):
    blocks = split_up(x, dim, lax.axis_size(axis))
    arrived = lax.all_to_all(blocks, axis, split_axis=0, concat_axis=0, tiled=True)
    return arrived.astype(jnp.float32).sum(axis=0)


def joined_along(blocks, dim):
    blocks = jnp.moveaxis(blocks, 0, dim)
    lengths = blocks.shape
    return blocks.reshape(*lengths[:dim], lengths[dim] * lengths[dim + 1], *lengths[dim + 2 :])


def gather_directly(x, axis, dim):
    return joined_along(sent_to_all(x, axis), dim)


def of_everyone(x, axis):
    return sent_to_all(x, axis).astype(jnp.float32).sum(axis=0)


def rms_scale(values, gain_vec, model_width):
    squares = taken_together(jnp.sum(values * values, axis=1), "ep")
    return values * lax.rsqrt(squares / model_width + EPSILON)[:, None] * gain_vec[None, :]


def to_heads(normed, weights):
    return sent_and_summed(
        jnp.dot(normed, weights, preferred_element_type=jnp.float32).astype(jnp.bfloat16), "ep", 0
    )


def from_heads(values, weights):
    partial_value = jnp.dot(
        gather_directly(values, "ep", 0), weights, preferred_element_type=jnp.float32
    )
    return (
        of_everyone(partial_value.astype(jnp.bfloat16), "tp")
        .astype(jnp.float32)
        .astype(jnp.bfloat16)
    )


def expert_terms(inputs, gate_w, up_w, down_w):
    gate_val = jnp.einsum("ecd,edf->ecf", inputs, gate_w, preferred_element_type=jnp.float32)
    up_val = jnp.einsum("ecd,edf->ecf", inputs, up_w, preferred_element_type=jnp.float32)
    hidden = (jax.nn.silu(gate_val) * up_val).astype(jnp.bfloat16)
    return jnp.einsum("ecf,efd->ecd", hidden, down_w, preferred_element_type=jnp.float32)


def slot_table(route_experts, experts, capacity):
    chosen = route_experts.reshape(-1)
    onehot = (chosen[:, None] == jnp.arange(experts, dtype=jnp.int32)[None, :]).astype(jnp.int32)
    earlier = jnp.cumsum(onehot, axis=0) - onehot
    rank_in = jnp.sum(earlier * onehot, axis=1)
    slot_ids = chosen * capacity + rank_in
    owners = jnp.arange(chosen.shape[0], dtype=jnp.int32) // route_experts.shape[1]
    filled = (
        jnp.full((experts * capacity,), route_experts.shape[0], jnp.int32).at[slot_ids].set(owners)
    )
    return (slot_ids, filled)


def per_device(
    stream,
    norm_gain,
    w_query,
    w_key,
    w_value,
    break_offset,
    cache_keys,
    cache_values,
    lengths,
    w_output,
    head_gain,
    ffn_gain,
    route_experts,
    route_weights,
    expert_gate,
    expert_up,
    expert_down,
    dense_gate,
    dense_up,
    dense_down,
    mix_gain,
):
    model_width = stream.shape[1] * lax.axis_size("ep")
    block_width = stream.shape[1]
    seq_count = lengths.shape[0]
    kv_local = cache_keys.shape[2]
    head_dim = cache_keys.shape[3]
    heads_local = break_offset.shape[0]
    group_size = heads_local // kv_local
    cache_len = cache_keys.shape[1]
    streamf = stream.astype(jnp.float32)
    normed = rms_scale(streamf, norm_gain, model_width).astype(jnp.bfloat16)
    projected = to_heads(normed, jnp.concatenate([w_query, w_key, w_value], axis=1))
    q_width = w_query.shape[1]
    k_width = w_key.shape[1]
    queries = (
        projected[:, :q_width]
        .astype(jnp.bfloat16)
        .reshape(seq_count, kv_local, group_size, head_dim)
    )
    key_rows = projected[:, q_width : q_width + k_width].astype(jnp.bfloat16)
    value_rows = projected[:, q_width + k_width :].astype(jnp.bfloat16)
    scores = jnp.einsum("skgd,slkd->skgl", queries, cache_keys, preferred_element_type=jnp.float32)
    scores = (
        scores * head_dim ** (-0.5) + break_offset.reshape(kv_local, group_size)[None, :, :, None]
    )
    in_cache = (jnp.arange(cache_len, dtype=jnp.int32)[None, :] < lengths[:, None])[
        :, None, None, :
    ]
    failed = jnp.where(in_cache, jax.nn.log_sigmoid(-scores), 0.0)
    later_sum = lax.cumsum(failed, axis=3, reverse=True) - failed
    weights = jnp.where(in_cache, jnp.exp(jax.nn.log_sigmoid(scores) + later_sum), 0.0).astype(
        jnp.bfloat16
    )
    attended = jnp.einsum(
        "skgl,slkd->skgd", weights, cache_values, preferred_element_type=jnp.float32
    )
    gains = head_gain.reshape(kv_local, group_size, head_dim)[None]
    normalized = (
        attended * lax.rsqrt(jnp.mean(attended * attended, axis=3, keepdims=True) + EPSILON) * gains
    )
    head_out = normalized.astype(jnp.bfloat16).reshape(seq_count, heads_local * head_dim)
    attn_out = from_heads(head_out, w_output)
    residual = streamf + attn_out.astype(jnp.float32)
    normed_ffn = rms_scale(residual, ffn_gain, model_width).astype(jnp.bfloat16)
    dense_width = dense_gate.shape[1]
    gate_up = to_heads(normed_ffn, jnp.concatenate([dense_gate, dense_up], axis=1))
    dense_hidden = (jax.nn.silu(gate_up[:, :dense_width]) * gate_up[:, dense_width:]).astype(
        jnp.bfloat16
    )
    dense_out = from_heads(dense_hidden, dense_down)
    experts = expert_gate.shape[0] * lax.axis_size("ep")
    capacity = 2 * seq_count * route_experts.shape[1] // expert_gate.shape[0]
    slot_ids, filled = slot_table(route_experts, experts, capacity)
    padded = jnp.concatenate([normed_ffn, jnp.zeros((1, block_width), jnp.bfloat16)], axis=0)
    outgoing = padded[filled].reshape(experts, capacity, block_width)
    slot_share = capacity // lax.axis_size("tp")
    own_slots = lax.dynamic_slice_in_dim(outgoing, lax.axis_index("tp") * slot_share, slot_share, 1)
    arrived = lax.all_to_all(own_slots, "ep", split_axis=0, concat_axis=2, tiled=True)
    gathered = lax.all_gather(arrived, "tp", axis=1, tiled=True)
    partial_value = expert_terms(gathered, expert_gate, expert_up, expert_down)
    summed = sent_and_summed(partial_value.astype(jnp.bfloat16), "tp", 1).astype(jnp.bfloat16)
    came_back = lax.all_to_all(summed, "ep", split_axis=2, concat_axis=0, tiled=True)
    returned = gather_directly(came_back, "tp", 1)
    picked = returned.reshape(experts * capacity, block_width)[slot_ids]
    picked = picked.reshape(route_experts.shape[0], route_experts.shape[1], block_width).astype(
        jnp.float32
    )
    shares = route_weights / jnp.sum(route_weights, axis=1, keepdims=True)
    moe_out = jnp.sum(picked * shares[:, :, None], axis=1)
    mixed_out = (residual + moe_out + mix_gain[None, :] * dense_out.astype(jnp.float32)).astype(
        jnp.bfloat16
    )
    return (mixed_out, key_rows, value_rows)


def solution(mesh):
    in_specs = (
        P(None, "ep"),
        P("ep"),
        P("ep", "tp"),
        P("ep", "tp"),
        P("ep", "tp"),
        P("tp"),
        P("ep", None, "tp", None),
        P("ep", None, "tp", None),
        P("ep"),
        P("tp", "ep"),
        P("tp"),
        P("ep"),
        P(),
        P(),
        P("ep", None, "tp"),
        P("ep", None, "tp"),
        P("ep", "tp", None),
        P("ep", "tp"),
        P("ep", "tp"),
        P("tp", "ep"),
        P("ep"),
    )
    out_specs = (P(None, "ep"), P("ep", "tp"), P("ep", "tp"))
    return jax.shard_map(
        per_device, mesh=mesh, in_specs=in_specs, out_specs=out_specs, check_vma=False
    )
```

profile of v0, /device:TPU:1, one launch (start us, length us, event | category | flops | bytes accessed | tf_op | source)
XLA Modules:
  0.0 309.1 jit_solution(11907331791318313063)
XLA Ops:
  1.8 20.5 %all_to_all.85 = f32[32,1,512]{2,1,0:T(1,128)S(1)} all-to-all(f32[32,1,512]{2,1,0:T(1,128)S(1)} %broadcast_in_dim.37), channel_id=1, replica_groups=mesh['ep'=32,'tp'=8] {'ep'}, dimensions={0} | all-to-all | bytes 131072 | tf_op jit(solution)/shard_map/all_to_all | solution.py:11
  24.5 3.9 %all-to-all-start.1 = ((bf16[32,16,512]{2,1,0:T(8,128)(2,1)}), bf16[32,16,512]{2,1,0:T(8,128)(2,1)S(1)}, u32[]{:S(2)}, u32[]{:S(2)}) async-start(bf16[32,16,512]{2,1,0:T(8,128)(2,1)} %bitcast), calls=%async_computation.1 | async-start | bytes 1048576 | tf_op jit(solution)/shard_map/all_to_all | solution.py:26
  29.1 14.2 %all-to-all-done.1 = bf16[32,16,512]{2,1,0:T(8,128)(2,1)S(1)} async-done(((bf16[32,16,512]{2,1,0:T(8,128)(2,1)}), bf16[32,16,512]{2,1,0:T(8,128)(2,1)S(1)}, u32[]{:S(2)}, u32[]{:S(2)}) %all-to-all-start.1) | async-done | bytes 524320 | tf_op jit(solution)/shard_map/all_to_all | solution.py:26
  47.0 39.6 %reduce-window.14 = f32[16,1,2,8,128]{4,3,2,1,0:T(8,128)S(1)} reduce-window(f32[16,1,2,8,128]{4,3,2,1,0:T(8,128)S(1)} %bitcast.111, f32[]{:T(128)} %constant.52.clone.1), window={size=1x1x1x1x128 pad=0_0x0_0x0_0x0_0x0_127}, to_apply=%region_3.4 | reduce-window | flops 4161536 | bytes 262148 | tf_op jit(solution)/shard_map/reduce-window
  91.3 6.3 %all-to-all-start.2 = ((bf16[32,16,256]{2,1,0:T(8,128)(2,1)}), bf16[32,16,256]{2,1,0:T(8,128)(2,1)S(1)}, u32[]{:S(2)}, u32[]{:S(2)}) async-start(bf16[32,16,256]{2,1,0:T(8,128)(2,1)} %broadcast_in_dim.39), calls=%async_computation.2 | async-start | bytes 524288 | tf_op jit(solution)/shard_map/all_to_all | solution.py:11
  98.0 10.1 %all-to-all-done.2 = bf16[32,16,256]{2,1,0:T(8,128)(2,1)S(1)} async-done(((bf16[32,16,256]{2,1,0:T(8,128)(2,1)}), bf16[32,16,256]{2,1,0:T(8,128)(2,1)S(1)}, u32[]{:S(2)}, u32[]{:S(2)}) %all-to-all-start.2) | async-done | bytes 262176 | tf_op jit(solution)/shard_map/all_to_all | solution.py:11
  109.4 8.2 %all-to-all-start.3 = ((bf16[8,512,128]{2,1,0:T(8,128)(2,1)}), bf16[8,512,128]{2,1,0:T(8,128)(2,1)S(1)}, u32[]{:S(2)}, u32[]{:S(2)}) async-start(bf16[8,512,128]{2,1,0:T(8,128)(2,1)} %broadcast_in_dim.40), calls=%async_computation.3 | async-start | bytes 2097152 | tf_op jit(solution)/shard_map/all_to_all | solution.py:11
  117.8 9.0 %reduce-window.16 = s32[32,8,128]{2,1,0:T(8,128)S(1)} reduce-window(s32[32,8,128]{2,1,0:T(8,128)S(1)} %fusion.43, s32[]{:T(128)} %constant.60.clone.1), window={size=1x1x128 pad=0_0x0_0x127_0}, to_apply=%region_9.10 | reduce-window | flops 4161536 | bytes 262148 | tf_op jit(solution)/shard_map/reduce-window.2
  127.7 4.3 %scatter_custom_fusion = s32[2048]{0:T(1024)S(1)} fusion(s32[1024]{0:T(1024)S(1)} %bitcast.121, s32[1024]{0:T(1024)S(1)} %add_select_fusion, s32[]{:T(128)} %constant.58.clone.1), kind=kCustom, calls=%fused_computation.86 | custom fusion | bytes 8196 | tf_op jit(solution)/shard_map/scatter | solution.py:81
  137.4 8.9 %all-to-all-done.4 = f32[32,1,512]{2,1,0:T(1,128)S(1)} async-done(((f32[32,1,512]{2,1,0:T(1,128)}), f32[32,1,512]{2,1,0:T(1,128)S(1)}, u32[]{:S(2)}, u32[]{:S(2)}) %all-to-all-start.4) | async-done | bytes 65568 | tf_op jit(solution)/shard_map/all_to_all | solution.py:11
  146.5 6.2 %gather_fusion = bf16[2048,128]{1,0:T(8,128)(2,1)S(1)} fusion(bf16[513,128]{1,0:T(8,128)(2,1)S(1)} %concatenate.10, s32[2048]{0:T(1024)S(1)} %fusion.52), kind=kCustom, calls=%fused_computation | custom fusion | bytes 1056768 | tf_op jit(solution)/shard_map/gather | solution.py:162
  152.8 12.0 %all_to_all.86 = bf16[32,8,128]{2,1,0:T(8,128)(2,1)S(1)} all-to-all(bf16[32,8,128]{2,1,0:T(8,128)(2,1)S(1)} %constant_dynamic-slice_fusion), channel_id=1, replica_groups=mesh['ep'=32,'tp'=8] {'ep'}, dimensions={0} | all-to-all | bytes 131072 | tf_op jit(solution)/shard_map/all_to_all | solution.py:165
  164.8 16.2 %all_gather.3 = bf16[1,64,4096]{2,1,0:T(8,128)(2,1)S(1)} all-gather(bf16[1,8,4096]{2,1,0:T(8,128)(2,1)S(1)} %bitcast.112), channel_id=1, replica_groups=mesh['ep'=32,'tp'=8] {'tp'}, dimensions={1}, use_global_device_ids=true | all-gather | bytes 589824 | tf_op jit(solution)/shard_map/all_gather | solution.py:166
  188.9 8.0 %all-to-all-done.6 = bf16[8,1,8,4096]{3,2,1,0:T(8,128)(2,1)S(1)} async-done(((bf16[8,1,8,4096]{3,2,1,0:T(8,128)(2,1)}), bf16[8,1,8,4096]{3,2,1,0:T(8,128)(2,1)S(1)}, u32[]{:S(2)}, u32[]{:S(2)}) %all-to-all-start.6) | async-done | bytes 524320 | tf_op jit(solution)/shard_map/all_to_all | solution.py:26
  196.9 4.8 %all-to-all-start.9 = ((bf16[32,16,1024]{2,1,0:T(8,128)(2,1)}), bf16[32,16,1024]{2,1,0:T(8,128)(2,1)}, u32[]{:S(2)}, u32[]{:S(2)}) async-start(bf16[32,16,1024]{2,1,0:T(8,128)(2,1)} %bitcast.28), calls=%async_computation.9 | async-start | bytes 2097152 | tf_op jit(solution)/shard_map/all_to_all | solution.py:26
  205.1 23.4 %reduce.9 = bf16[4096,8]{1,0:T(8,128)(2,1)} reduce(bf16[4096,1,8]{2,1,0:T(2,128)(2,1)S(1)} %bitcast.103, bf16[]{:T(256)} %broadcast.165), dimensions={1}, to_apply=%bitcast.86.reduce_sub_computation | reduce | bytes 131074
  231.6 9.1 %all-to-all-start.7 = ((bf16[32,2,512]{2,1,0:T(2,128)(2,1)}), bf16[32,2,512]{2,1,0:T(2,128)(2,1)S(1)}, u32[]{:S(2)}, u32[]{:S(2)}) async-start(bf16[32,2,512]{2,1,0:T(2,128)(2,1)} %reshape.282), calls=%async_computation.7 | async-start | bytes 131072 | tf_op jit(solution)/shard_map/all_to_all | solution.py:169
  242.2 7.4 %all-to-all-done.7 = bf16[32,2,512]{2,1,0:T(2,128)(2,1)S(1)} async-done(((bf16[32,2,512]{2,1,0:T(2,128)(2,1)}), bf16[32,2,512]{2,1,0:T(2,128)(2,1)S(1)}, u32[]{:S(2)}, u32[]{:S(2)}) %all-to-all-start.7) | async-done | bytes 65568 | tf_op jit(solution)/shard_map/all_to_all | solution.py:169
  250.4 4.6 %all-to-all-start.10 = ((bf16[32,16,512]{2,1,0:T(8,128)(2,1)}), bf16[32,16,512]{2,1,0:T(8,128)(2,1)}, u32[]{:S(2)}, u32[]{:S(2)}) async-start(bf16[32,16,512]{2,1,0:T(8,128)(2,1)} %broadcast_in_dim.46), calls=%async_computation.10 | async-start | bytes 1048576 | tf_op jit(solution)/shard_map/all_to_all | solution.py:11
  259.8 9.4 %all-to-all-done.10 = bf16[32,16,512]{2,1,0:T(8,128)(2,1)} async-done(((bf16[32,16,512]{2,1,0:T(8,128)(2,1)}), bf16[32,16,512]{2,1,0:T(8,128)(2,1)}, u32[]{:S(2)}, u32[]{:S(2)}) %all-to-all-start.10) | async-done | bytes 524320 | tf_op jit(solution)/shard_map/all_to_all | solution.py:11
  270.1 8.2 %all-to-all-start.8 = ((bf16[8,32,8,128]{3,2,1,0:T(8,128)(2,1)}), bf16[8,32,8,128]{3,2,1,0:T(8,128)(2,1)S(1)}, u32[]{:S(2)}, u32[]{:S(2)}) async-start(bf16[8,32,8,128]{3,2,1,0:T(8,128)(2,1)} %broadcast_in_dim.45), calls=%async_computation.8 | async-start | bytes 1048576 | tf_op jit(solution)/shard_map/all_to_all | solution.py:11
  279.6 8.0 %all-to-all-done.8 = bf16[8,32,8,128]{3,2,1,0:T(8,128)(2,1)S(1)} async-done(((bf16[8,32,8,128]{3,2,1,0:T(8,128)(2,1)}), bf16[8,32,8,128]{3,2,1,0:T(8,128)(2,1)S(1)}, u32[]{:S(2)}, u32[]{:S(2)}) %all-to-all-start.8) | async-done | bytes 524320 | tf_op jit(solution)/shard_map/all_to_all | solution.py:11
  288.8 4.4 %all-to-all-start.11 = ((bf16[8,512,128]{2,1,0:T(8,128)(2,1)}), bf16[8,512,128]{2,1,0:T(8,128)(2,1)S(1)}, u32[]{:S(2)}, u32[]{:S(2)}) async-start(bf16[8,512,128]{2,1,0:T(8,128)(2,1)} %broadcast_in_dim.47), calls=%async_computation.11 | async-start | bytes 2097152 | tf_op jit(solution)/shard_map/all_to_all | solution.py:11
  301.8 6.4 %all-to-all-done.11 = bf16[8,512,128]{2,1,0:T(8,128)(2,1)S(1)} async-done(((bf16[8,512,128]{2,1,0:T(8,128)(2,1)}), bf16[8,512,128]{2,1,0:T(8,128)(2,1)S(1)}, u32[]{:S(2)}, u32[]{:S(2)}) %all-to-all-start.11) | async-done | bytes 1048608 | tf_op jit(solution)/shard_map/all_to_all | solution.py:11
  (103 shorter events, 54.9 us)
Async XLA Ops:
  0.6 181.9 %copy-start = (bf16[1,128,4096]{2,1,0:T(8,128)(2,1)S(1)}, bf16[1,128,4096]{2,1,0:T(8,128)(2,1)}, u32[]{:S(2)}) copy-start(bf16[1,128,4096]{2,1,0:T(8,128)(2,1)} %param.37) | copy-start | bytes 3145732
  24.5 18.8 %all-to-all-start.1 = ((bf16[32,16,512]{2,1,0:T(8,128)(2,1)}), bf16[32,16,512]{2,1,0:T(8,128)(2,1)S(1)}, u32[]{:S(2)}, u32[]{:S(2)}) async-start(bf16[32,16,512]{2,1,0:T(8,128)(2,1)} %bitcast), calls=%async_computation.1 | async-start | bytes 1048576 | tf_op jit(solution)/shard_map/all_to_all | solution.py:26
  46.8 43.6 %copy-start.8 = (f32[256]{0:T(256)S(1)}, f32[256]{0:T(256)}, u32[]{:S(2)}) copy-start(f32[256]{0:T(256)} %param.31) | copy-start | bytes 3076
  46.8 50.8 %copy-start.6 = (s32[512,2]{0,1:T(2,128)S(1)}, s32[512,2]{0,1:T(2,128)}, u32[]{:S(2)}) copy-start(s32[512,2]{0,1:T(2,128)} %param.33) | copy-start | bytes 12292
  46.9 61.1 %copy-start.5 = (bf16[256,128]{1,0:T(8,128)(2,1)S(1)}, bf16[256,128]{1,0:T(8,128)(2,1)}, u32[]{:S(2)}) copy-start(bf16[256,128]{1,0:T(8,128)(2,1)} %param.30) | copy-start | bytes 196612
  90.5 42.2 %copy-start.1 = (bf16[512,128]{1,0:T(8,128)(2,1)S(1)}, bf16[512,128]{1,0:T(8,128)(2,1)}, u32[]{:S(2)}) copy-start(bf16[512,128]{1,0:T(8,128)(2,1)} %param.21) | copy-start | bytes 393220
  91.3 55.1 %copy-start.9 = (f32[128]{0:T(128)S(1)}, f32[128]{0:T(128)}, u32[]{:S(2)}) copy-start(f32[128]{0:T(128)} %param.32) | copy-start | bytes 1540
  91.3 16.7 %all-to-all-start.2 = ((bf16[32,16,256]{2,1,0:T(8,128)(2,1)}), bf16[32,16,256]{2,1,0:T(8,128)(2,1)S(1)}, u32[]{:S(2)}, u32[]{:S(2)}) async-start(bf16[32,16,256]{2,1,0:T(8,128)(2,1)} %broadcast_in_dim.39), calls=%async_computation.2 | async-start | bytes 524288 | tf_op jit(solution)/shard_map/all_to_all | solution.py:11
  109.4 23.2 %all-to-all-start.3 = ((bf16[8,512,128]{2,1,0:T(8,128)(2,1)}), bf16[8,512,128]{2,1,0:T(8,128)(2,1)S(1)}, u32[]{:S(2)}, u32[]{:S(2)}) async-start(bf16[8,512,128]{2,1,0:T(8,128)(2,1)} %broadcast_in_dim.40), calls=%async_computation.3 | async-start | bytes 2097152 | tf_op jit(solution)/shard_map/all_to_all | solution.py:11
  132.7 49.8 %copy-start.2 = (bf16[1,4096,128]{2,1,0:T(8,128)(2,1)S(1)}, bf16[1,4096,128]{2,1,0:T(8,128)(2,1)}, u32[]{:S(2)}) copy-start(bf16[1,4096,128]{2,1,0:T(8,128)(2,1)} %param.36) | copy-start | bytes 3145732
  133.6 12.7 %all-to-all-start.4 = ((f32[32,1,512]{2,1,0:T(1,128)}), f32[32,1,512]{2,1,0:T(1,128)S(1)}, u32[]{:S(2)}, u32[]{:S(2)}) async-start(f32[32,1,512]{2,1,0:T(1,128)} %broadcast_in_dim.41), calls=%async_computation.4 | async-start | bytes 131072 | tf_op jit(solution)/shard_map/all_to_all | solution.py:11
  152.7 34.8 %copy-start.3 = (bf16[128,512]{1,0:T(8,128)(2,1)S(1)}, bf16[128,512]{1,0:T(8,128)(2,1)}, u32[]{:S(2)}) copy-start(bf16[128,512]{1,0:T(8,128)(2,1)} %param.39) | copy-start | bytes 393220
  152.7 34.8 %copy-start.4 = (bf16[128,512]{1,0:T(8,128)(2,1)S(1)}, bf16[128,512]{1,0:T(8,128)(2,1)}, u32[]{:S(2)}) copy-start(bf16[128,512]{1,0:T(8,128)(2,1)} %param.38) | copy-start | bytes 393220
  183.9 12.9 %all-to-all-start.6 = ((bf16[8,1,8,4096]{3,2,1,0:T(8,128)(2,1)}), bf16[8,1,8,4096]{3,2,1,0:T(8,128)(2,1)S(1)}, u32[]{:S(2)}, u32[]{:S(2)}) async-start(bf16[8,1,8,4096]{3,2,1,0:T(8,128)(2,1)} %fusion), calls=%async_computation.6 | async-start | bytes 1048576 | tf_op jit(solution)/shard_map/all_to_all | solution.py:26
  196.9 34.7 %all-to-all-start.9 = ((bf16[32,16,1024]{2,1,0:T(8,128)(2,1)}), bf16[32,16,1024]{2,1,0:T(8,128)(2,1)}, u32[]{:S(2)}, u32[]{:S(2)}) async-start(bf16[32,16,1024]{2,1,0:T(8,128)(2,1)} %bitcast.28), calls=%async_computation.9 | async-start | bytes 2097152 | tf_op jit(solution)/shard_map/all_to_all | solution.py:26
  231.6 18.0 %all-to-all-start.7 = ((bf16[32,2,512]{2,1,0:T(2,128)(2,1)}), bf16[32,2,512]{2,1,0:T(2,128)(2,1)S(1)}, u32[]{:S(2)}, u32[]{:S(2)}) async-start(bf16[32,2,512]{2,1,0:T(2,128)(2,1)} %reshape.282), calls=%async_computation.7 | async-start | bytes 131072 | tf_op jit(solution)/shard_map/all_to_all | solution.py:169
  250.4 18.8 %all-to-all-start.10 = ((bf16[32,16,512]{2,1,0:T(8,128)(2,1)}), bf16[32,16,512]{2,1,0:T(8,128)(2,1)}, u32[]{:S(2)}, u32[]{:S(2)}) async-start(bf16[32,16,512]{2,1,0:T(8,128)(2,1)} %broadcast_in_dim.46), calls=%async_computation.10 | async-start | bytes 1048576 | tf_op jit(solution)/shard_map/all_to_all | solution.py:11
  257.9 35.4 %copy-start.7 = (f32[512,2]{0,1:T(2,128)S(1)}, f32[512,2]{0,1:T(2,128)}, u32[]{:S(2)}) copy-start(f32[512,2]{0,1:T(2,128)} %param.34) | copy-start | bytes 12292
  270.1 17.6 %all-to-all-start.8 = ((bf16[8,32,8,128]{3,2,1,0:T(8,128)(2,1)}), bf16[8,32,8,128]{3,2,1,0:T(8,128)(2,1)S(1)}, u32[]{:S(2)}, u32[]{:S(2)}) async-start(bf16[8,32,8,128]{3,2,1,0:T(8,128)(2,1)} %broadcast_in_dim.45), calls=%async_computation.8 | async-start | bytes 1048576 | tf_op jit(solution)/shard_map/all_to_all | solution.py:11
  279.6 28.7 %copy-start.10 = (f32[128]{0:T(128)S(1)}, f32[128]{0:T(128)}, u32[]{:S(2)}) copy-start(f32[128]{0:T(128)} %param.41) | copy-start | bytes 1540
  288.8 19.4 %all-to-all-start.11 = ((bf16[8,512,128]{2,1,0:T(8,128)(2,1)}), bf16[8,512,128]{2,1,0:T(8,128)(2,1)S(1)}, u32[]{:S(2)}, u32[]{:S(2)}) async-start(bf16[8,512,128]{2,1,0:T(8,128)(2,1)} %broadcast_in_dim.47), calls=%async_computation.11 | async-start | bytes 2097152 | tf_op jit(solution)/shard_map/all_to_all | solution.py:11
where the time goes:
time: 310 us; the launch traced here: 309 us
  other arithmetic  81 us (26%)
  waiting for transfers between devices  72.8 us (23%)
  starting transfers between devices  57.1 us (18%)
  blocking collectives  48.7 us (16%)
  local copies, waits for them, and re-layouts  33.7 us (11%)
  matrix products  14.7 us (5%)
    another operation x5, other arithmetic  48.8 us
    all_to_all x6, waiting for transfers between devices, sent_to_all(): lax.all_to_all(jnp.broadcast_to(x[None], (size, *x.shape)), axis, 0, 0, t...  43.3 us
    all_to_all x6, starting transfers between devices, sent_to_all(): lax.all_to_all(jnp.broadcast_to(x[None], (size, *x.shape)), axis, 0, 0, t...  35.6 us
    unnamed x1, other arithmetic  23.4 us
    all_to_all x3, waiting for transfers between devices, sent_and_summed(): lax.all_to_all(blocks, axis, split_axis=0, concat_axis=0, tiled=True)  22.1 us
    all_to_all x1, blocking collectives, sent_to_all(): lax.all_to_all(jnp.broadcast_to(x[None], (size, *x.shape)), axis, 0, 0, t...  20.5 us
    all_gather x1, blocking collectives, per_device(): gathered = lax.all_gather(arrived, 'tp', axis=1, tiled=True)  16.2 us
    all_to_all x3, starting transfers between devices, sent_and_summed(): lax.all_to_all(blocks, axis, split_axis=0, concat_axis=0, tiled=True)  12.3 us
  transfers between devices with their start and end apart: 10, of which 9 were waited for; matrix products, arithmetic and copies ran while one was open for 20% of the time, Pallas kernels for 0%

commit v1 on v0

--- a/solution.py
+++ b/solution.py
@@ -163,7 +163,21 @@
     slot_share = capacity // lax.axis_size("tp")
     own_slots = lax.dynamic_slice_in_dim(outgoing, lax.axis_index("tp") * slot_share, slot_share, 1)
     arrived = lax.all_to_all(own_slots, "ep", split_axis=0, concat_axis=2, tiled=True)
-    gathered = lax.all_gather(arrived, "tp", axis=1, tiled=True)
+    ways, here, step = (lax.axis_size("tp"), lax.axis_index("tp"), arrived.shape[1])
+    dims = [n * ways if d == 1 else n for d, n in enumerate(arrived.shape)]
+    full = lax.dynamic_update_slice_in_dim(
+        jnp.zeros(dims, arrived.dtype), arrived, here * step, axis=1
+    )
+    going_up = going_down = arrived
+    for far in range(1, ways // 2 + 1):
+        going_up = lax.ppermute(going_up, "tp", [(d, (d + 1) % ways) for d in range(ways)])
+        full = lax.dynamic_update_slice_in_dim(full, going_up, (here - far) % ways * step, axis=1)
+        if 2 * far < ways:
+            going_down = lax.ppermute(going_down, "tp", [(d, (d - 1) % ways) for d in range(ways)])
+            full = lax.dynamic_update_slice_in_dim(
+                full, going_down, (here + far) % ways * step, axis=1
+            )
+    gathered = full
     partial_value = expert_terms(gathered, expert_gate, expert_up, expert_down)
     summed = sent_and_summed(partial_value.astype(jnp.bfloat16), "tp", 1).astype(jnp.bfloat16)
     came_back = lax.all_to_all(summed, "ep", split_axis=2, concat_axis=0, tiled=True)

time: 310 us -> 318 us (1.026)
  blocking collectives: 48.7 us -> 20.5 us
  starting transfers between devices: 57.1 us -> 76 us
  waiting for transfers between devices: 72.8 us -> 89 us
    all_gather x1 -> x0, blocking collectives: 16.2 us -> none  [per_device(): gathered = lax.all_gather(arrived, 'tp', axis=1, tiled=True)]
    all_to_all x1 -> x0, blocking collectives: 12 us -> none  [per_device(): lax.all_to_all(own_slots, 'ep', split_axis=0, concat_axis=2, tiled=True)]
    ppermute x0 -> x7, starting transfers between devices: none -> 11.1 us  [the longest x4 8.39 us: per_device(): lax.ppermute(going_up, 'tp', [(d, (d + 1) % ways) for d in range(ways)])]
    all_to_all x0 -> x1, waiting for transfers between devices: none -> 8.74 us  [per_device(): lax.all_to_all(own_slots, 'ep', split_axis=0, concat_axis=2, tiled=True)]
    ppermute x0 -> x7, waiting for transfers between devices: none -> 7.46 us  [the longest x4 6.59 us: per_device(): lax.ppermute(going_up, 'tp', [(d, (d + 1) % ways) for d in range(ways)])]
    all_to_all x3, starting transfers between devices: 12.3 us -> 16.3 us  [sent_and_summed(): lax.all_to_all(blocks, axis, split_axis=0, concat_axis=0, tiled=True)]
    all_to_all x0 -> x1, starting transfers between devices: none -> 3.86 us  [per_device(): lax.all_to_all(own_slots, 'ep', split_axis=0, concat_axis=2, tiled=True)]
  transfers between devices with their start and end apart: 10 -> 18, of which waited for: 9 -> 17; matrix products, arithmetic and copies ran while one was open for 20% -> 20% of each run, Pallas kernels for 0% -> 0%
where the time goes in v1:
time: 318 us; the launch traced here: 317 us
  waiting for transfers between devices  89 us (28%)
  other arithmetic  81 us (25%)
  starting transfers between devices  76 us (24%)
  local copies, waits for them, and re-layouts  34.4 us (11%)
  blocking collectives  20.5 us (6%)
  matrix products  14.7 us (5%)
    another operation x5, other arithmetic  48.8 us
    all_to_all x6, waiting for transfers between devices, sent_to_all(): lax.all_to_all(jnp.broadcast_to(x[None], (size, *x.shape)), axis, 0, 0, t...  43.3 us
    all_to_all x6, starting transfers between devices, sent_to_all(): lax.all_to_all(jnp.broadcast_to(x[None], (size, *x.shape)), axis, 0, 0, t...  35.6 us
    unnamed x1, other arithmetic  23.4 us
    all_to_all x3, waiting for transfers between devices, sent_and_summed(): lax.all_to_all(blocks, axis, split_axis=0, concat_axis=0, tiled=True)  22.1 us
    all_to_all x1, blocking collectives, sent_to_all(): lax.all_to_all(jnp.broadcast_to(x[None], (size, *x.shape)), axis, 0, 0, t...  20.5 us
    all_to_all x3, starting transfers between devices, sent_and_summed(): lax.all_to_all(blocks, axis, split_axis=0, concat_axis=0, tiled=True)  16.3 us
    all_to_all x1, starting transfers between devices, per_device(): lax.all_to_all(summed, 'ep', split_axis=2, concat_axis=0, tiled=True)  9.14 us
  transfers between devices with their start and end apart: 18, of which 17 were waited for; matrix products, arithmetic and copies ran while one was open for 20% of the time, Pallas kernels for 0%

profile of v1, /device:TPU:1, one launch (start us, length us, event | category | flops | bytes accessed | tf_op | source)
XLA Modules:
  0.0 317.0 jit_solution(4911465647891334685)
XLA Ops:
  1.8 20.5 %all_to_all.85 = f32[32,1,512]{2,1,0:T(1,128)S(1)} all-to-all(f32[32,1,512]{2,1,0:T(1,128)S(1)} %broadcast_in_dim.37), channel_id=1, replica_groups=mesh['ep'=32,'tp'=8] {'ep'}, dimensions={0} | all-to-all | bytes 131072 | tf_op jit(solution)/shard_map/all_to_all | solution.py:11
  29.1 14.2 %all-to-all-done.1 = bf16[32,16,512]{2,1,0:T(8,128)(2,1)S(1)} async-done(((bf16[32,16,512]{2,1,0:T(8,128)(2,1)}), bf16[32,16,512]{2,1,0:T(8,128)(2,1)S(1)}, u32[]{:S(2)}, u32[]{:S(2)}) %all-to-all-start.1) | async-done | bytes 524320 | tf_op jit(solution)/shard_map/all_to_all | solution.py:26
  47.0 39.6 %reduce-window.14 = f32[16,1,2,8,128]{4,3,2,1,0:T(8,128)S(1)} reduce-window(f32[16,1,2,8,128]{4,3,2,1,0:T(8,128)S(1)} %bitcast.127, f32[]{:T(128)} %constant.101.clone.1), window={size=1x1x1x1x128 pad=0_0x0_0x0_0x0_0x0_127}, to_apply=%region_3.4 | reduce-window | flops 4161536 | bytes 262148 | tf_op jit(solution)/shard_map/reduce-window
  91.3 6.3 %all-to-all-start.2 = ((bf16[32,16,256]{2,1,0:T(8,128)(2,1)}), bf16[32,16,256]{2,1,0:T(8,128)(2,1)S(1)}, u32[]{:S(2)}, u32[]{:S(2)}) async-start(bf16[32,16,256]{2,1,0:T(8,128)(2,1)} %broadcast_in_dim.39), calls=%async_computation.2 | async-start | bytes 524288 | tf_op jit(solution)/shard_map/all_to_all | solution.py:11
  98.0 10.1 %all-to-all-done.2 = bf16[32,16,256]{2,1,0:T(8,128)(2,1)S(1)} async-done(((bf16[32,16,256]{2,1,0:T(8,128)(2,1)}), bf16[32,16,256]{2,1,0:T(8,128)(2,1)S(1)}, u32[]{:S(2)}, u32[]{:S(2)}) %all-to-all-start.2) | async-done | bytes 262176 | tf_op jit(solution)/shard_map/all_to_all | solution.py:11
  109.4 8.2 %all-to-all-start.3 = ((bf16[8,512,128]{2,1,0:T(8,128)(2,1)}), bf16[8,512,128]{2,1,0:T(8,128)(2,1)S(1)}, u32[]{:S(2)}, u32[]{:S(2)}) async-start(bf16[8,512,128]{2,1,0:T(8,128)(2,1)} %broadcast_in_dim.40), calls=%async_computation.3 | async-start | bytes 2097152 | tf_op jit(solution)/shard_map/all_to_all | solution.py:11
  117.8 9.0 %reduce-window.16 = s32[32,8,128]{2,1,0:T(8,128)S(1)} reduce-window(s32[32,8,128]{2,1,0:T(8,128)S(1)} %fusion.39, s32[]{:T(128)} %constant.109.clone.1), window={size=1x1x128 pad=0_0x0_0x127_0}, to_apply=%region_9.10 | reduce-window | flops 4161536 | bytes 262148 | tf_op jit(solution)/shard_map/reduce-window.2
  127.7 4.3 %scatter_custom_fusion = s32[2048]{0:T(1024)S(1)} fusion(s32[1024]{0:T(1024)S(1)} %bitcast.138, s32[1024]{0:T(1024)S(1)} %add_select_fusion, s32[]{:T(128)} %constant.107.clone.1), kind=kCustom, calls=%fused_computation.87 | custom fusion | bytes 8196 | tf_op jit(solution)/shard_map/scatter | solution.py:81
  137.4 8.9 %all-to-all-done.4 = f32[32,1,512]{2,1,0:T(1,128)S(1)} async-done(((f32[32,1,512]{2,1,0:T(1,128)}), f32[32,1,512]{2,1,0:T(1,128)S(1)}, u32[]{:S(2)}, u32[]{:S(2)}) %all-to-all-start.4) | async-done | bytes 65568 | tf_op jit(solution)/shard_map/all_to_all | solution.py:11
  146.5 6.2 %gather_fusion = bf16[2048,128]{1,0:T(8,128)(2,1)S(1)} fusion(bf16[513,128]{1,0:T(8,128)(2,1)S(1)} %concatenate.10, s32[2048]{0:T(1024)S(1)} %fusion.47), kind=kCustom, calls=%fused_computation | custom fusion | bytes 1056768 | tf_op jit(solution)/shard_map/gather | solution.py:162
  157.4 8.7 %all-to-all-done.5 = bf16[32,8,128]{2,1,0:T(8,128)(2,1)S(1)} async-done(((bf16[32,8,128]{2,1,0:T(8,128)(2,1)}), bf16[32,8,128]{2,1,0:T(8,128)(2,1)S(1)}, u32[]{:S(2)}, u32[]{:S(2)}) %all-to-all-start.5) | async-done | bytes 65568 | tf_op jit(solution)/shard_map/all_to_all | solution.py:165
  181.0 3.9 %collective-permute-done.6 = bf16[1,8,4096]{2,1,0:T(8,128)(2,1)S(1)} collective-permute-done((bf16[1,8,4096]{2,1,0:T(8,128)(2,1)S(1)}, bf16[1,8,4096]{2,1,0:T(8,128)(2,1)S(1)}, u32[]{:S(2)}, u32[]{:S(2)}) %collective-permute-start.6) | collective-permute-done | bytes 65568 | tf_op jit(solution)/shard_map/ppermute | solution.py:173
  187.9 7.5 %all-to-all-start.6 = ((bf16[8,1,8,4096]{3,2,1,0:T(8,128)(2,1)}), bf16[8,1,8,4096]{3,2,1,0:T(8,128)(2,1)S(1)}, u32[]{:S(2)}, u32[]{:S(2)}) async-start(bf16[8,1,8,4096]{3,2,1,0:T(8,128)(2,1)} %fusion), calls=%async_computation.6 | async-start | bytes 1048576 | tf_op jit(solution)/shard_map/all_to_all | solution.py:26
  196.8 8.0 %all-to-all-done.6 = bf16[8,1,8,4096]{3,2,1,0:T(8,128)(2,1)S(1)} async-done(((bf16[8,1,8,4096]{3,2,1,0:T(8,128)(2,1)}), bf16[8,1,8,4096]{3,2,1,0:T(8,128)(2,1)S(1)}, u32[]{:S(2)}, u32[]{:S(2)}) %all-to-all-start.6) | async-done | bytes 524320 | tf_op jit(solution)/shard_map/all_to_all | solution.py:26
  204.8 4.8 %all-to-all-start.9 = ((bf16[32,16,1024]{2,1,0:T(8,128)(2,1)}), bf16[32,16,1024]{2,1,0:T(8,128)(2,1)}, u32[]{:S(2)}, u32[]{:S(2)}) async-start(bf16[32,16,1024]{2,1,0:T(8,128)(2,1)} %bitcast.37), calls=%async_computation.9 | async-start | bytes 2097152 | tf_op jit(solution)/shard_map/all_to_all | solution.py:26
  213.0 23.4 %reduce.9 = bf16[4096,8]{1,0:T(8,128)(2,1)} reduce(bf16[4096,1,8]{2,1,0:T(2,128)(2,1)S(1)} %bitcast.119, bf16[]{:T(256)} %broadcast.181), dimensions={1}, to_apply=%bitcast.100.reduce_sub_computation | reduce | bytes 131074
  239.5 9.1 %all-to-all-start.7 = ((bf16[32,2,512]{2,1,0:T(2,128)(2,1)}), bf16[32,2,512]{2,1,0:T(2,128)(2,1)S(1)}, u32[]{:S(2)}, u32[]{:S(2)}) async-start(bf16[32,2,512]{2,1,0:T(2,128)(2,1)} %reshape.320), calls=%async_computation.7 | async-start | bytes 131072 | tf_op jit(solution)/shard_map/all_to_all | solution.py:183
  250.1 7.4 %all-to-all-done.7 = bf16[32,2,512]{2,1,0:T(2,128)(2,1)S(1)} async-done(((bf16[32,2,512]{2,1,0:T(2,128)(2,1)}), bf16[32,2,512]{2,1,0:T(2,128)(2,1)S(1)}, u32[]{:S(2)}, u32[]{:S(2)}) %all-to-all-start.7) | async-done | bytes 65568 | tf_op jit(solution)/shard_map/all_to_all | solution.py:183
  258.4 4.6 %all-to-all-start.10 = ((bf16[32,16,512]{2,1,0:T(8,128)(2,1)}), bf16[32,16,512]{2,1,0:T(8,128)(2,1)}, u32[]{:S(2)}, u32[]{:S(2)}) async-start(bf16[32,16,512]{2,1,0:T(8,128)(2,1)} %broadcast_in_dim.46), calls=%async_computation.10 | async-start | bytes 1048576 | tf_op jit(solution)/shard_map/all_to_all | solution.py:11
  267.7 9.4 %all-to-all-done.10 = bf16[32,16,512]{2,1,0:T(8,128)(2,1)} async-done(((bf16[32,16,512]{2,1,0:T(8,128)(2,1)}), bf16[32,16,512]{2,1,0:T(8,128)(2,1)}, u32[]{:S(2)}, u32[]{:S(2)}) %all-to-all-start.10) | async-done | bytes 524320 | tf_op jit(solution)/shard_map/all_to_all | solution.py:11
  278.0 8.2 %all-to-all-start.8 = ((bf16[8,32,8,128]{3,2,1,0:T(8,128)(2,1)}), bf16[8,32,8,128]{3,2,1,0:T(8,128)(2,1)S(1)}, u32[]{:S(2)}, u32[]{:S(2)}) async-start(bf16[8,32,8,128]{3,2,1,0:T(8,128)(2,1)} %broadcast_in_dim.45), calls=%async_computation.8 | async-start | bytes 1048576 | tf_op jit(solution)/shard_map/all_to_all | solution.py:11
  287.6 8.0 %all-to-all-done.8 = bf16[8,32,8,128]{3,2,1,0:T(8,128)(2,1)S(1)} async-done(((bf16[8,32,8,128]{3,2,1,0:T(8,128)(2,1)}), bf16[8,32,8,128]{3,2,1,0:T(8,128)(2,1)S(1)}, u32[]{:S(2)}, u32[]{:S(2)}) %all-to-all-start.8) | async-done | bytes 524320 | tf_op jit(solution)/shard_map/all_to_all | solution.py:11
  296.7 4.4 %all-to-all-start.11 = ((bf16[8,512,128]{2,1,0:T(8,128)(2,1)}), bf16[8,512,128]{2,1,0:T(8,128)(2,1)S(1)}, u32[]{:S(2)}, u32[]{:S(2)}) async-start(bf16[8,512,128]{2,1,0:T(8,128)(2,1)} %broadcast_in_dim.47), calls=%async_computation.11 | async-start | bytes 2097152 | tf_op jit(solution)/shard_map/all_to_all | solution.py:11
  309.7 6.4 %all-to-all-done.11 = bf16[8,512,128]{2,1,0:T(8,128)(2,1)S(1)} async-done(((bf16[8,512,128]{2,1,0:T(8,128)(2,1)}), bf16[8,512,128]{2,1,0:T(8,128)(2,1)S(1)}, u32[]{:S(2)}, u32[]{:S(2)}) %all-to-all-start.11) | async-done | bytes 1048608 | tf_op jit(solution)/shard_map/all_to_all | solution.py:11
  (126 shorter events, 74.5 us)
Async XLA Ops:
  0.6 185.8 %copy-start = (bf16[1,128,4096]{2,1,0:T(8,128)(2,1)S(1)}, bf16[1,128,4096]{2,1,0:T(8,128)(2,1)}, u32[]{:S(2)}) copy-start(bf16[1,128,4096]{2,1,0:T(8,128)(2,1)} %param.37) | copy-start | bytes 3145732
  24.5 18.8 %all-to-all-start.1 = ((bf16[32,16,512]{2,1,0:T(8,128)(2,1)}), bf16[32,16,512]{2,1,0:T(8,128)(2,1)S(1)}, u32[]{:S(2)}, u32[]{:S(2)}) async-start(bf16[32,16,512]{2,1,0:T(8,128)(2,1)} %bitcast), calls=%async_computation.1 | async-start | bytes 1048576 | tf_op jit(solution)/shard_map/all_to_all | solution.py:26
  46.8 43.6 %copy-start.8 = (f32[256]{0:T(256)S(1)}, f32[256]{0:T(256)}, u32[]{:S(2)}) copy-start(f32[256]{0:T(256)} %param.31) | copy-start | bytes 3076
  46.8 50.8 %copy-start.6 = (s32[512,2]{0,1:T(2,128)S(1)}, s32[512,2]{0,1:T(2,128)}, u32[]{:S(2)}) copy-start(s32[512,2]{0,1:T(2,128)} %param.33) | copy-start | bytes 12292
  46.9 61.1 %copy-start.5 = (bf16[256,128]{1,0:T(8,128)(2,1)S(1)}, bf16[256,128]{1,0:T(8,128)(2,1)}, u32[]{:S(2)}) copy-start(bf16[256,128]{1,0:T(8,128)(2,1)} %param.30) | copy-start | bytes 196612
  91.3 55.1 %copy-start.9 = (f32[128]{0:T(128)S(1)}, f32[128]{0:T(128)}, u32[]{:S(2)}) copy-start(f32[128]{0:T(128)} %param.32) | copy-start | bytes 1540
  91.3 16.7 %all-to-all-start.2 = ((bf16[32,16,256]{2,1,0:T(8,128)(2,1)}), bf16[32,16,256]{2,1,0:T(8,128)(2,1)S(1)}, u32[]{:S(2)}, u32[]{:S(2)}) async-start(bf16[32,16,256]{2,1,0:T(8,128)(2,1)} %broadcast_in_dim.39), calls=%async_computation.2 | async-start | bytes 524288 | tf_op jit(solution)/shard_map/all_to_all | solution.py:11
  109.4 23.2 %all-to-all-start.3 = ((bf16[8,512,128]{2,1,0:T(8,128)(2,1)}), bf16[8,512,128]{2,1,0:T(8,128)(2,1)S(1)}, u32[]{:S(2)}, u32[]{:S(2)}) async-start(bf16[8,512,128]{2,1,0:T(8,128)(2,1)} %broadcast_in_dim.40), calls=%async_computation.3 | async-start | bytes 2097152 | tf_op jit(solution)/shard_map/all_to_all | solution.py:11
  133.5 12.7 %all-to-all-start.4 = ((f32[32,1,512]{2,1,0:T(1,128)}), f32[32,1,512]{2,1,0:T(1,128)S(1)}, u32[]{:S(2)}, u32[]{:S(2)}) async-start(f32[32,1,512]{2,1,0:T(1,128)} %broadcast_in_dim.41), calls=%async_computation.4 | async-start | bytes 131072 | tf_op jit(solution)/shard_map/all_to_all | solution.py:11
  152.7 42.7 %copy-start.3 = (bf16[128,512]{1,0:T(8,128)(2,1)S(1)}, bf16[128,512]{1,0:T(8,128)(2,1)}, u32[]{:S(2)}) copy-start(bf16[128,512]{1,0:T(8,128)(2,1)} %param.39) | copy-start | bytes 393220
  153.4 12.7 %all-to-all-start.5 = ((bf16[32,8,128]{2,1,0:T(8,128)(2,1)}), bf16[32,8,128]{2,1,0:T(8,128)(2,1)S(1)}, u32[]{:S(2)}, u32[]{:S(2)}) async-start(bf16[32,8,128]{2,1,0:T(8,128)(2,1)} %constant_dynamic-slice_fusion), calls=%async_computation.5 | async-start | bytes 131072 | tf_op jit(solution)/shard_map/all_to_all | solution.py:165
  166.1 4.8 %collective-permute-start = (bf16[1,8,4096]{2,1,0:T(8,128)(2,1)S(1)}, bf16[1,8,4096]{2,1,0:T(8,128)(2,1)S(1)}, u32[]{:S(2)}, u32[]{:S(2)}) collective-permute-start(bf16[1,8,4096]{2,1,0:T(8,128)(2,1)S(1)} %bitcast.129), channel_id=1, source_target_pairs={{0,1},{1,2},{2,3},{3,4},{4,5},{5,6},{6,7},{7,0},{8,9},{9,10},{10,1... | collective-permute-start | bytes 196616 | tf_op jit(solution)/shard_map/ppermute | solution.py:173
  169.6 4.0 %collective-permute-start.1 = (bf16[1,8,4096]{2,1,0:T(8,128)(2,1)S(1)}, bf16[1,8,4096]{2,1,0:T(8,128)(2,1)S(1)}, u32[]{:S(2)}, u32[]{:S(2)}) collective-permute-start(bf16[1,8,4096]{2,1,0:T(8,128)(2,1)S(1)} %bitcast.130), channel_id=1, source_target_pairs={{0,7},{1,0},{2,1},{3,2},{4,3},{5,4},{6,5},{7,6},{8,15},{9,8},{10,9... | collective-permute-start | bytes 196616 | tf_op jit(solution)/shard_map/ppermute | solution.py:176
  170.9 4.1 %collective-permute-start.2 = (bf16[1,8,4096]{2,1,0:T(8,128)(2,1)S(1)}, bf16[1,8,4096]{2,1,0:T(8,128)(2,1)S(1)}, u32[]{:S(2)}, u32[]{:S(2)}) collective-permute-start(bf16[1,8,4096]{2,1,0:T(8,128)(2,1)S(1)} %collective-permute-done), channel_id=1, source_target_pairs={{0,1},{1,2},{2,3},{3,4},{4,5},{5,6},{6,7},{7,0},{8,9},{9,10},{10,1... | collective-permute-start | bytes 196616 | tf_op jit(solution)/shard_map/ppermute | solution.py:173
  173.6 3.7 %collective-permute-start.3 = (bf16[1,8,4096]{2,1,0:T(8,128)(2,1)S(1)}, bf16[1,8,4096]{2,1,0:T(8,128)(2,1)S(1)}, u32[]{:S(2)}, u32[]{:S(2)}) collective-permute-start(bf16[1,8,4096]{2,1,0:T(8,128)(2,1)S(1)} %collective-permute-done.1), channel_id=1, source_target_pairs={{0,7},{1,0},{2,1},{3,2},{4,3},{5,4},{6,5},{7,6},{8,15},{9,8},{10,9... | collective-permute-start | bytes 196616 | tf_op jit(solution)/shard_map/ppermute | solution.py:176
  175.1 4.9 %collective-permute-start.4 = (bf16[1,8,4096]{2,1,0:T(8,128)(2,1)S(1)}, bf16[1,8,4096]{2,1,0:T(8,128)(2,1)S(1)}, u32[]{:S(2)}, u32[]{:S(2)}) collective-permute-start(bf16[1,8,4096]{2,1,0:T(8,128)(2,1)S(1)} %collective-permute-done.2), channel_id=1, source_target_pairs={{0,1},{1,2},{2,3},{3,4},{4,5},{5,6},{6,7},{7,0},{8,9},{9,10},{10,1... | collective-permute-start | bytes 196616 | tf_op jit(solution)/shard_map/ppermute | solution.py:173
  177.3 3.7 %collective-permute-start.5 = (bf16[1,8,4096]{2,1,0:T(8,128)(2,1)S(1)}, bf16[1,8,4096]{2,1,0:T(8,128)(2,1)S(1)}, u32[]{:S(2)}, u32[]{:S(2)}) collective-permute-start(bf16[1,8,4096]{2,1,0:T(8,128)(2,1)S(1)} %collective-permute-done.3), channel_id=1, source_target_pairs={{0,7},{1,0},{2,1},{3,2},{4,3},{5,4},{6,5},{7,6},{8,15},{9,8},{10,9... | collective-permute-start | bytes 196616 | tf_op jit(solution)/shard_map/ppermute | solution.py:176
  180.0 4.9 %collective-permute-start.6 = (bf16[1,8,4096]{2,1,0:T(8,128)(2,1)S(1)}, bf16[1,8,4096]{2,1,0:T(8,128)(2,1)S(1)}, u32[]{:S(2)}, u32[]{:S(2)}) collective-permute-start(bf16[1,8,4096]{2,1,0:T(8,128)(2,1)S(1)} %collective-permute-done.4), channel_id=1, source_target_pairs={{0,1},{1,2},{2,3},{3,4},{4,5},{5,6},{6,7},{7,0},{8,9},{9,10},{10,1... | collective-permute-start | bytes 196616 | tf_op jit(solution)/shard_map/ppermute | solution.py:173
  187.9 16.9 %all-to-all-start.6 = ((bf16[8,1,8,4096]{3,2,1,0:T(8,128)(2,1)}), bf16[8,1,8,4096]{3,2,1,0:T(8,128)(2,1)S(1)}, u32[]{:S(2)}, u32[]{:S(2)}) async-start(bf16[8,1,8,4096]{3,2,1,0:T(8,128)(2,1)} %fusion), calls=%async_computation.6 | async-start | bytes 1048576 | tf_op jit(solution)/shard_map/all_to_all | solution.py:26
  204.8 34.7 %all-to-all-start.9 = ((bf16[32,16,1024]{2,1,0:T(8,128)(2,1)}), bf16[32,16,1024]{2,1,0:T(8,128)(2,1)}, u32[]{:S(2)}, u32[]{:S(2)}) async-start(bf16[32,16,1024]{2,1,0:T(8,128)(2,1)} %bitcast.37), calls=%async_computation.9 | async-start | bytes 2097152 | tf_op jit(solution)/shard_map/all_to_all | solution.py:26
  239.5 18.0 %all-to-all-start.7 = ((bf16[32,2,512]{2,1,0:T(2,128)(2,1)}), bf16[32,2,512]{2,1,0:T(2,128)(2,1)S(1)}, u32[]{:S(2)}, u32[]{:S(2)}) async-start(bf16[32,2,512]{2,1,0:T(2,128)(2,1)} %reshape.320), calls=%async_computation.7 | async-start | bytes 131072 | tf_op jit(solution)/shard_map/all_to_all | solution.py:183
  258.4 18.8 %all-to-all-start.10 = ((bf16[32,16,512]{2,1,0:T(8,128)(2,1)}), bf16[32,16,512]{2,1,0:T(8,128)(2,1)}, u32[]{:S(2)}, u32[]{:S(2)}) async-start(bf16[32,16,512]{2,1,0:T(8,128)(2,1)} %broadcast_in_dim.46), calls=%async_computation.10 | async-start | bytes 1048576 | tf_op jit(solution)/shard_map/all_to_all | solution.py:11
  278.0 17.6 %all-to-all-start.8 = ((bf16[8,32,8,128]{3,2,1,0:T(8,128)(2,1)}), bf16[8,32,8,128]{3,2,1,0:T(8,128)(2,1)S(1)}, u32[]{:S(2)}, u32[]{:S(2)}) async-start(bf16[8,32,8,128]{3,2,1,0:T(8,128)(2,1)} %broadcast_in_dim.45), calls=%async_computation.8 | async-start | bytes 1048576 | tf_op jit(solution)/shard_map/all_to_all | solution.py:11
  296.7 19.4 %all-to-all-start.11 = ((bf16[8,512,128]{2,1,0:T(8,128)(2,1)}), bf16[8,512,128]{2,1,0:T(8,128)(2,1)S(1)}, u32[]{:S(2)}, u32[]{:S(2)}) async-start(bf16[8,512,128]{2,1,0:T(8,128)(2,1)} %broadcast_in_dim.47), calls=%async_computation.11 | async-start | bytes 2097152 | tf_op jit(solution)/shard_map/all_to_all | solution.py:11
  (5 other events, 188.8 us)
